TPU v7x, 32 devices: a whole 2x2x4 slice. The times are simulated.
32 devices in a mesh: row: 8 (over z, core), col: 4 (over y, x).
Axes of the slice: x: 2, y: 2, z: 4, core: 2. Of those that a mesh axis runs over, the one named last changes fastest.
Arguments:
- mix_input: bfloat16 [4, 2048, 1024], P('col', 'row'), may hold values from -6 to 6
- gate_logits: bfloat16 [4, 2048, 2048], P('col', 'row'), may hold values from -8 to 8
- w_proj: bfloat16 [1024, 2048], P('col'), may hold values from -0.1875 to 0.1875
Outputs:
- mixed: bfloat16 [4, 2048, 2048], P('col', 'row')
All inputs are finite; a program needn't handle non-finite values.
Results may differ from a plain program's by a relative error of at most 0.0049.
Values may be sent and summed in bfloat16 or wider, within the bound.
A program may use at most 64 MiB of HBM per device.

v0:
```python
import math

import jax
import jax.numpy as jnp
from jax import lax
from jax.sharding import PartitionSpec as P

GROUP = 256
GROUPS = 4
POS_INNER = 128


highest = lax.Precision.HIGHEST


def tables(rows_in, cols_out, period):
    left_index = jnp.arange(rows_in, dtype=jnp.int32)[:, None]
    right_index = jnp.arange(cols_out, dtype=jnp.int32)[None, :]
    angles = (left_index * right_index % period).astype(jnp.float32) * (2.0 * math.pi / period)
    return (jnp.cos(angles), jnp.sin(angles))


def half_tables(group_size):
    index_row = jnp.arange(group_size, dtype=jnp.int32)
    frequency = jnp.where(index_row == 1, group_size // 2, index_row // 2)
    is_cosine = jnp.logical_or(index_row % 2 == 0, index_row == 1)
    channel = jnp.arange(group_size, dtype=jnp.int32)[:, None]
    angles = (channel * frequency[None, :] % group_size).astype(jnp.float32) * (
        2.0 * math.pi / group_size
    )
    return jnp.where(is_cosine[None, :], jnp.cos(angles), jnp.sin(angles))


def position_transform(values, inner_len):
    length, columns = values.shape
    outer_len = length // inner_len
    blocks = values.reshape(inner_len, outer_len, columns)
    cos_one, sin_one = tables(inner_len, inner_len, inner_len)
    first_re = jnp.einsum("pqc,pk->ckq", blocks, cos_one, precision=highest)
    first_im = -jnp.einsum("pqc,pk->ckq", blocks, sin_one, precision=highest)
    cos_twist, sin_twist = tables(inner_len, outer_len, length)
    second_re = first_re * cos_twist + first_im * sin_twist
    second_im = first_im * cos_twist - first_re * sin_twist
    cos_two, sin_two = tables(outer_len, outer_len, outer_len)
    whole_re = jnp.einsum("ckq,qj->cjk", second_re, cos_two, precision=highest) + jnp.einsum(
        "ckq,qj->cjk", second_im, sin_two, precision=highest
    )
    whole_im = jnp.einsum("ckq,qj->cjk", second_im, cos_two, precision=highest) - jnp.einsum(
        "ckq,qj->cjk", second_re, sin_two, precision=highest
    )
    return (whole_re.reshape(columns, length), whole_im.reshape(columns, length))


def on_device(mix_input, gate_logits, w_proj):
    tokens = mix_input[0]
    tok_count, features = tokens.shape
    row_count = lax.axis_size("row")
    length = tok_count * row_count
    norm_factor = 1.0 / math.sqrt(length * GROUP)
    grouped = tokens.astype(jnp.float32).reshape(tok_count, GROUPS, GROUP)
    packed = jnp.einsum("tgc,cm->tgm", grouped, half_tables(GROUP), precision=highest).reshape(
        tok_count, features
    )
    packed_cols = lax.all_to_all(packed, "row", split_axis=1, concat_axis=0, tiled=True)
    part_re, part_im = position_transform(packed_cols, POS_INNER)
    columns = part_re.shape[0]
    pair_re = part_re.reshape(columns // 2, 2, length)
    pair_im = part_im.reshape(columns // 2, 2, length)
    pair_index = lax.axis_index("row") * (columns // 2) + jnp.arange(columns // 2, dtype=jnp.int32)
    special = (pair_index % (GROUP // 2) == 0)[:, None]
    low_half = jnp.where(special, pair_re[:, 0], pair_re[:, 0] + pair_im[:, 1])
    high_half = jnp.where(special, pair_re[:, 1], pair_re[:, 0] - pair_im[:, 1])
    paired = (
        jnp.stack([low_half, high_half], axis=1).reshape(columns, length) * norm_factor
    ).astype(jnp.bfloat16)
    returned = lax.all_to_all(paired, "row", split_axis=1, concat_axis=0, tiled=True)
    pair_grid = returned.reshape(GROUPS, GROUP // 2, 2, tok_count)
    spectrum = jnp.concatenate(
        [pair_grid[:, :, 0], pair_grid[:, :1, 1], jnp.flip(pair_grid[:, 1:, 1], axis=1)], axis=1
    ).reshape(features, tok_count)
    projected = lax.dot_general(
        spectrum,
        lax.all_gather(w_proj, "col", axis=0, tiled=True),
        (((0,), (0,)), ((), ())),
        preferred_element_type=jnp.float32,
    )
    gate_open = jax.nn.sigmoid(gate_logits[0].astype(jnp.float32))
    return (gate_open * projected).astype(jnp.bfloat16)[None]


def solution(mesh):
    in_specs = (P("col", "row", None), P("col", "row", None), P("col", None))
    out_specs = P("col", "row", None)
    return jax.shard_map(
        on_device, mesh=mesh, in_specs=in_specs, out_specs=out_specs, check_vma=False
    )
```

profile of v0, /device:TPU:1, one launch (start us, length us, event | category | flops | bytes accessed | tf_op | source)
XLA Modules:
  0.0 90.6 jit_solution(6947621169780344983)
XLA Ops:
  6.5 0.7 all-gather.2.cloned.1.call-update
  7.3 1.4 %reshape.125 = bf16[256,4,256]{2,1,0:T(4,128)(2,1)S(1)} reshape(bf16[1,256,1024]{2,1,0:T(8,128)(2,1)} %param.3) | data formatting | bytes 1048576 | tf_op jit(solution)/shard_map/reshape | solution.py:60
  8.7 1.7 %fusion.8 = f32[256,256,4]{1,0,2:T(8,128)S(1)} fusion(bf16[256,4,256]{2,1,0:T(4,128)(2,1)S(1)} %reshape.125, s32[256]{0:T(256)S(1)} %fusion.67, pred[256]{0:T(512)(128)(4,1)S(1)} %compare_or_fusion), kind=kOutput, calls=%fused_computation.18 | convolution fusion | flops 806289408 | bytes 1574144 | tf_op jit(solution)/shard_map/tgc,cm->tgm/dot_general | solution.py:61
  10.4 1.3 %copy.30 = f32[256,8,128]{2,0,1:T(8,128)} copy(f32[256,8,128]{0,2,1:T(8,128)S(1)} %bitcast.61) | data formatting | bytes 2097152 | tf_op jit(solution)/shard_map/all_to_all | solution.py:64
  11.7 6.4 %all-to-all-start = ((f32[256,8,128]{2,0,1:T(8,128)}), f32[256,8,128]{2,0,1:T(8,128)S(1)}, u32[]{:S(2)}, u32[]{:S(2)}) async-start(f32[256,8,128]{2,0,1:T(8,128)} %copy.30), calls=%async_computation | async-start | bytes 2097152 | tf_op jit(solution)/shard_map/all_to_all | solution.py:64
  18.2 25.5 %all-to-all-done = f32[256,8,128]{2,0,1:T(8,128)S(1)} async-done(((f32[256,8,128]{2,0,1:T(8,128)}), f32[256,8,128]{2,0,1:T(8,128)S(1)}, u32[]{:S(2)}, u32[]{:S(2)}) %all-to-all-start) | async-done | bytes 1048608 | tf_op jit(solution)/shard_map/all_to_all | solution.py:64
  43.7 1.5 %convolution_negate_fusion = f32[128,16,128]{2,0,1:T(8,128)S(1)} fusion(f32[128,16,128]{2,1,0:T(8,128)S(1)} %bitcast.56), kind=kOutput, calls=%fused_computation.7 | convolution fusion | flops 403144704 | bytes 2097152 | tf_op jit(solution)/shard_map/pqc,pk->ckq/dot_general | solution.py:40
  45.2 2.8 %subtract_bitcast_fusion = (f32[128,128,16]{0,1,2:T(8,128)S(1)}, f32[128,128,16]{0,1,2:T(8,128)}) fusion(f32[128,16,128]{2,0,1:T(8,128)S(1)} %convolution_negate_fusion, f32[128,16]{0,1:T(8,128)S(1)} %get-tuple-element.9, f32[128,16]{0,1:T(8,128)S(1)} %get-tuple-element.10, f32[128,16,128]{2,1,0:T(8,128)S(1)} %bitcast.57), kind=kOutput, calls=%fused_computation.10 | convolution fusion | flops 404455424 | bytes 4210688 | tf_op jit(solution)/shard_map/pqc,pk->ckq/dot_general | solution.py:39
  48.0 1.7 %copy.33 = f32[128,128,16]{1,2,0:T(8,128)S(1)} copy(f32[128,128,16]{0,1,2:T(8,128)} %get-tuple-element.6) | data formatting | bytes 2097152 | tf_op jit(solution)/shard_map/add | solution.py:42
  49.7 0.5 copy.34
  50.2 1.0 %fusion.51 = f32[16,128,128]{2,0,1:T(8,128)S(1)} fusion(f32[128,128,16]{1,2,0:T(8,128)S(1)} %copy.33), kind=kOutput, calls=%fused_computation.70 | convolution fusion | flops 50335232 | bytes 2097152 | tf_op jit(solution)/shard_map/ckq,qj->cjk/dot_general | solution.py:45
  51.2 1.1 %fusion.3 = f32[128,16,128]{2,1,0:T(8,128)S(1)} fusion(f32[16,128,128]{2,0,1:T(8,128)S(1)} %fusion.51, f32[128,128,16]{1,2,0:T(8,128)S(1)} %copy.34), kind=kOutput, calls=%fused_computation.6 | convolution fusion | flops 50597376 | bytes 3145728 | tf_op jit(solution)/shard_map/ckq,qj->cjk/dot_general | solution.py:45
  52.3 1.5 %reshape_reshape.6 = f32[64,2,2048]{2,1,0:T(2,128)} reshape(f32[128,16,128]{2,1,0:T(8,128)S(1)} %fusion.3) | data formatting | bytes 2097152 | tf_op jit(solution)/shard_map/reshape;reshape | solution.py:67
  53.8 1.0 %fusion.49 = f32[16,128,128]{2,0,1:T(8,128)S(1)} fusion(f32[128,128,16]{1,2,0:T(8,128)S(1)} %copy.34), kind=kOutput, calls=%fused_computation.68 | convolution fusion | flops 50335232 | bytes 2097152 | tf_op jit(solution)/shard_map/ckq,qj->cjk/dot_general | solution.py:48
  54.9 1.1 %fusion.2 = f32[128,16,128]{2,1,0:T(8,128)S(1)} fusion(f32[16,128,128]{2,0,1:T(8,128)S(1)} %fusion.49, f32[128,128,16]{1,2,0:T(8,128)S(1)} %copy.33), kind=kOutput, calls=%fused_computation.4 | convolution fusion | flops 50597376 | bytes 3145728 | tf_op jit(solution)/shard_map/ckq,qj->cjk/dot_general | solution.py:48
  56.0 0.5 reshape_reshape.7
  56.6 1.6 %broadcast_select_fusion.1 = (f32[64,1,2048]{2,1,0:T(1,128)S(1)}, f32[64,1,2048]{2,1,0:T(1,128)S(1)}) fusion(pred[64]{0:T(512)(128)(4,1)S(1)} %fusion.69, f32[64,2,2048]{2,1,0:T(2,128)S(1)} %reshape_reshape.7, f32[64,2,2048]{2,1,0:T(2,128)S(1)} %copy-done), kind=kLoop, calls=%fused_computation.13 | loop fusion | flops 524288 | bytes 2621504 | tf_op jit(solution)/shard_map/jit(_where)/select_n | solution.py:71
  58.1 1.1 %fusion.4 = bf16[64,2,2048]{2,1,0:T(2,128)(2,1)S(1)} fusion(f32[64,1,2048]{2,1,0:T(1,128)S(1)} %get-tuple-element.8, f32[64,1,2048]{2,1,0:T(1,128)S(1)} %get-tuple-element.7), kind=kLoop, calls=%fused_computation.9 | loop fusion | flops 786432 | bytes 1572864 | tf_op jit(solution)/shard_map/convert_element_type | solution.py:75
  59.3 0.3 convert_element_type.54
  59.7 17.9 %all_to_all.29 = bf16[128,8,256]{2,0,1:T(8,128)(2,1)S(1)} all-to-all(bf16[128,8,256]{2,0,1:T(8,128)(2,1)S(1)} %copy.37), channel_id=1, replica_groups=mesh['row'=8,'col'=4] {'row'}, dimensions={1} | all-to-all | bytes 1048576 | tf_op jit(solution)/shard_map/all_to_all | solution.py:76
  77.6 0.2 reshape.127
  77.8 0.6 slice.32
  78.4 0.5 rev.4
  79.1 4.6 %fusion.1 = bf16[1,256,2048]{2,1,0:T(8,128)(2,1)} fusion(bf16[1024,256]{1,0:T(8,128)(2,1)S(1)} %bitcast.63, bf16[1024,2048]{1,0:T(8,128)(2,1)} %all-gather.2.cloned.1.call-done, bf16[1,256,2048]{2,1,0:T(8,128)(2,1)S(1)} %copy-done.1), kind=kOutput, calls=%fused_computation.2 | convolution fusion | flops 1076887552 | bytes 6815744 | tf_op jit(solution)/shard_map/dot_general | solution.py:81
  (15 shorter events, 0.4 us)
Async XLA Ops:
  6.5 72.5 %all-gather.2.cloned.1.call-start = ((), (), s32[]{:S(2)}) async-start(), calls=%async_computation.2 | async-start | bytes 5242880 | tf_op jit(solution)/shard_map/all_gather | solution.py:83
  11.7 32.0 %all-to-all-start = ((f32[256,8,128]{2,0,1:T(8,128)}), f32[256,8,128]{2,0,1:T(8,128)S(1)}, u32[]{:S(2)}, u32[]{:S(2)}) async-start(f32[256,8,128]{2,0,1:T(8,128)} %copy.30), calls=%async_computation | async-start | bytes 2097152 | tf_op jit(solution)/shard_map/all_to_all | solution.py:64
  54.9 1.7 %copy-start = (f32[64,2,2048]{2,1,0:T(2,128)S(1)}, f32[64,2,2048]{2,1,0:T(2,128)}, u32[]{:S(2)}) copy-start(f32[64,2,2048]{2,1,0:T(2,128)} %reshape_reshape.6) | copy-start | bytes 3145732
  77.8 1.3 %copy-start.1 = (bf16[1,256,2048]{2,1,0:T(8,128)(2,1)S(1)}, bf16[1,256,2048]{2,1,0:T(8,128)(2,1)}, u32[]{:S(2)}) copy-start(bf16[1,256,2048]{2,1,0:T(8,128)(2,1)} %param.4) | copy-start | bytes 3145732
Sparse Core Ops, SparseCore 0:
  9.2 54.4 all-gather.1
where the time goes:
time: 91.9 us; the launch traced here: 90.6 us
  waiting for transfers between devices  26.3 us (29%)
  blocking collectives  17.9 us (19%)
  matrix products  14.9 us (16%)
  between operations  13.6 us (15%)
  local copies, waits for them, and re-layouts  8.74 us (10%)
  starting transfers between devices  6.37 us (7%)
  other arithmetic  2.85 us (3%)
    all_to_all x1, waiting for transfers between devices, on_device(): lax.all_to_all(packed, 'row', split_axis=1, concat_axis=0, tiled=True)  25.5 us
    all_to_all x1, blocking collectives, on_device(): lax.all_to_all(paired, 'row', split_axis=1, concat_axis=0, tiled=True)  17.9 us
    all_to_all x1, starting transfers between devices, on_device(): lax.all_to_all(packed, 'row', split_axis=1, concat_axis=0, tiled=True)  6.37 us
    dot_general x1, matrix products, on_device(): lax.dot_general(spectrum, lax.all_gather(w_proj, 'col', axis=0, tiled=Tru...  4.64 us
    dot_general x1, matrix products, position_transform(): first_re = jnp.einsum('pqc,pk->ckq', blocks, cos_one, precision=highest)  2.84 us
  transfers between devices with their start and end apart: 2, of which 1 were waited for; matrix products, arithmetic and copies ran while one was open for 24% of the time, Pallas kernels for 0%

commit v1 on v0

--- a/solution.py
+++ b/solution.py
@@ -1,9 +1,17 @@
+import functools
 import math
 
 import jax
 import jax.numpy as jnp
+import numpy as np
 from jax import lax
+from jax.experimental import pallas as pl
+from jax.experimental.pallas import tpu as pltpu
 from jax.sharding import PartitionSpec as P
+
+MESH = pl.DeviceIdType.MESH
+TAB_STEP = 32
+OUT_CHUNK = 512
 
 GROUP = 256
 GROUPS = 4
@@ -88,9 +96,382 @@
     return (gate_open * projected).astype(jnp.bfloat16)[None]
 
 
+def channel_table(rows):
+    half = GROUP // 2
+    quarter = half // 2
+    table = np.zeros((GROUP, GROUP))
+    mixing = np.zeros((GROUP, GROUP))
+    channel = np.arange(GROUP)
+    for core in range(2):
+        for i in range(quarter):
+            m = quarter * core + i
+            low, high = half * core + i, half * core + quarter + i
+            angle = 2.0 * np.pi * (channel * m % GROUP) / GROUP
+            table[:, low] = np.cos(angle)
+            table[:, high] = np.sin(angle) if m else np.cos(np.pi * channel)
+            mixing[low, m] = 1.0
+            mixing[high, GROUP - m if m else half] = 1.0
+    return table, mixing
+
+
+def base_tables(length):
+    position = np.arange(length)
+    coarse = np.arange(length // 2 // TAB_STEP)[:, None] * TAB_STEP
+    fine = np.arange(TAB_STEP)[:, None]
+    step = 2.0 * np.pi / length
+    coarse_angle = (coarse * position % length) * step
+    fine_angle = (fine * position % length) * step
+    return (
+        np.stack([np.cos(coarse_angle), np.sin(coarse_angle)]).astype(np.float32),
+        np.stack([np.cos(fine_angle), np.sin(fine_angle)]).astype(np.float32),
+    )
+
+
+def fused_kernel(
+    rows,
+    cols,
+    norm_factor,
+    x_hbm,
+    gate_hbm,
+    w_hbm,
+    chan_hbm,
+    mix_hbm,
+    coarse_hbm,
+    fine_hbm,
+    out_hbm,
+    xv,
+    gv,
+    wv,
+    chan,
+    mix,
+    coarse,
+    fine,
+    send_x,
+    recv_x,
+    tab,
+    rhs,
+    send_y,
+    spec,
+    wall,
+    sig,
+    outv,
+    load_sem,
+    out_sem,
+    sx,
+    rx,
+    sy,
+    ry,
+    sw,
+    rw,
+    sf,
+    rf,
+):
+    f32, bf16 = jnp.float32, jnp.bfloat16
+    row, col = lax.axis_index("row"), lax.axis_index("col")
+    chip, core = row // 2, row % 2
+    tok = xv.shape[0]
+    width = recv_x.shape[1]
+    length = recv_x.shape[0]
+    half_len = length // 2
+    half_rows = GROUP // 2
+
+    loads = [
+        pltpu.make_async_copy(src, dst, load_sem.at[i])
+        for i, (src, dst) in enumerate(
+            [
+                (x_hbm, xv),
+                (chan_hbm, chan),
+                (w_hbm, wv),
+                (mix_hbm, mix),
+                (coarse_hbm, coarse),
+                (fine_hbm, fine),
+                (gate_hbm, gv),
+            ]
+        )
+    ]
+    for load in loads:
+        load.start()
+
+    barrier = pltpu.get_barrier_semaphore()
+    for i in range(1, rows):
+        pl.semaphore_signal(
+            barrier, inc=1, device_id=(lax.rem(row + i, rows), col), device_id_type=MESH
+        )
+    for i in range(1, cols):
+        pl.semaphore_signal(
+            barrier, inc=1, device_id=(row, lax.rem(col + i, cols)), device_id_type=MESH
+        )
+
+    def x_copy(dest, source):
+        return pltpu.make_async_remote_copy(
+            src_ref=send_x.at[dest],
+            dst_ref=recv_x.at[pl.ds(pl.multiple_of(source * tok, tok), tok), :],
+            send_sem=sx.at[dest],
+            recv_sem=rx.at[source],
+            device_id=(dest, col),
+            device_id_type=MESH,
+        )
+
+    def y_copy(dest, source):
+        return pltpu.make_async_remote_copy(
+            src_ref=send_y.at[dest],
+            dst_ref=spec.at[:, pl.ds(pl.multiple_of(source * width, width), width)],
+            send_sem=sy.at[dest],
+            recv_sem=ry.at[source],
+            device_id=(dest, col),
+            device_id_type=MESH,
+        )
+
+    def w_part(owner, part):
+        return wall.at[owner, pl.ds(pl.multiple_of(part * half_rows, half_rows), half_rows), :]
+
+    def w_copy(dest, owner):
+        return pltpu.make_async_remote_copy(
+            src_ref=w_part(owner, core),
+            dst_ref=w_part(owner, core),
+            send_sem=sw.at[dest],
+            recv_sem=rw.at[owner],
+            device_id=(row, dest),
+            device_id_type=MESH,
+        )
+
+    def f_copy(owner, part):
+        return pltpu.make_async_remote_copy(
+            src_ref=w_part(owner, part),
+            dst_ref=w_part(owner, part),
+            send_sem=sf.at[owner],
+            recv_sem=rf.at[owner],
+            device_id=(row + 1 - 2 * core, col),
+            device_id_type=MESH,
+        )
+
+    loads[0].wait()
+    loads[1].wait()
+    pl.semaphore_wait(barrier, rows - 1 + cols - 1)
+
+    for i in range(GROUPS):
+        g = lax.rem(chip + GROUPS // 2 + i, GROUPS)
+        packed = jnp.dot(
+            xv[:, pl.ds(pl.multiple_of(g * GROUP, GROUP), GROUP)],
+            chan[...],
+            preferred_element_type=f32,
+        ).astype(bf16)
+        for part in range(2):
+            dest = 2 * g + part
+            block = packed[:, part * width : (part + 1) * width]
+
+            @pl.when(dest != row)
+            def _():
+                send_x[dest] = block
+                x_copy(dest, row).start()
+
+            @pl.when(dest == row)
+            def _():
+                recv_x[pl.ds(pl.multiple_of(row * tok, tok), tok), :] = block
+
+    loads[2].wait()
+    loads[3].wait()
+    wall[col] = jnp.dot(mix[...], wv[...], preferred_element_type=f32).astype(bf16)
+    for i in range(1, cols):
+        w_copy(lax.rem(col + i, cols), col).start()
+
+    loads[4].wait()
+    loads[5].wait()
+
+    def make_rows(a, carry):
+        at = pl.ds(pl.multiple_of(a * TAB_STEP, TAB_STEP), TAB_STEP)
+        for n in range(0, length, 512):
+            cc = coarse[0, pl.ds(a, 1), n : n + 512]
+            cs = coarse[1, pl.ds(a, 1), n : n + 512]
+            fc = fine[0, :, n : n + 512]
+            fs = fine[1, :, n : n + 512]
+            tab[at, n : n + 512] = (cc * fc - cs * fs).astype(bf16)
+            tab[at, length + n : length + n + 512] = (cs * fc + cc * fs).astype(bf16)
+        return carry
+
+    lax.fori_loop(0, half_len // TAB_STEP, make_rows, 0)
+
+    loads[6].wait()
+
+    def open_gate(i, carry):
+        at = pl.ds(pl.multiple_of(i * 16, 16), 16)
+        sig[at, :] = jax.nn.sigmoid(gv[at, :].astype(f32))
+        return carry
+
+    lax.fori_loop(0, tok // 16, open_gate, 0)
+
+    quarter = width // 2
+    left = lax.broadcasted_iota(jnp.int32, (width, width), 0)
+    right = lax.broadcasted_iota(jnp.int32, (width, width), 1)
+    first = jnp.logical_and(core == 0, right % quarter == 0)
+    cos_from = jnp.where(first, right, right % quarter)
+    cos_pick = jnp.where(left == cos_from, 1.0, 0.0).astype(bf16)
+    sign = jnp.where(first, 0.0, jnp.where(right < quarter, -1.0, 1.0))
+    sin_pick = jnp.where(left == right % quarter + quarter, sign, 0.0).astype(bf16)
+    odd = lax.broadcasted_iota(jnp.int32, (tok, width), 0) % 2
+    flip = jnp.where(odd == 1, -1.0, 1.0)
+
+    for i in range(rows):
+        source = lax.rem(row + i, rows)
+
+        @pl.when(source != row)
+        def _():
+            x_copy(source, source).wait_recv()
+
+        at = pl.ds(pl.multiple_of(source * tok, tok), tok)
+        block = recv_x[at, :]
+        for base, pick in ((0, cos_pick), (length, sin_pick)):
+            picked = jnp.dot(block, pick, preferred_element_type=f32)
+            to = pl.ds(pl.multiple_of(base + source * tok, tok), tok)
+            rhs[to, :width] = picked.astype(bf16)
+            rhs[to, width:] = (picked * flip).astype(bf16)
+
+    def position_block(e, carry):
+        at = pl.ds(pl.multiple_of(e * tok, tok), tok)
+        block = jnp.dot(tab[at, :], rhs[...], preferred_element_type=f32) * norm_factor
+        block = block.astype(bf16)
+        for part in range(2):
+            dest = e + part * (rows // 2)
+            piece = block[:, part * width : (part + 1) * width]
+
+            @pl.when(dest != row)
+            def _():
+                send_y[dest] = piece
+                y_copy(dest, row).start()
+
+            @pl.when(dest == row)
+            def _():
+                spec[:, pl.ds(pl.multiple_of(row * width, width), width)] = piece
+
+        return carry
+
+    lax.fori_loop(0, rows // 2, position_block, 0)
+
+    for i in range(1, cols):
+        owner = lax.rem(col + i, cols)
+        w_copy(owner, owner).wait_recv()
+        f_copy(owner, core).start()
+
+    for i in range(1, rows):
+        source = lax.rem(row + i, rows)
+        y_copy(source, source).wait_recv()
+    for i in range(1, cols):
+        owner = lax.rem(col + i, cols)
+        f_copy(owner, 1 - core).wait_recv()
+
+    chunks = outv.shape[1] // OUT_CHUNK
+
+    def out_copy(j):
+        at = pl.ds(pl.multiple_of(j * OUT_CHUNK, OUT_CHUNK), OUT_CHUNK)
+        return pltpu.make_async_copy(outv.at[:, at], out_hbm.at[:, at], out_sem.at[j])
+
+    def project(j, carry):
+        at = pl.ds(pl.multiple_of(j * OUT_CHUNK, OUT_CHUNK), OUT_CHUNK)
+        total = jnp.zeros((tok, OUT_CHUNK), f32)
+        for g in range(GROUPS):
+            total += jnp.dot(
+                spec[:, g * GROUP : (g + 1) * GROUP], wall[g, :, at], preferred_element_type=f32
+            )
+        outv[:, at] = (sig[:, at] * total).astype(bf16)
+        out_copy(j).start()
+        return carry
+
+    lax.fori_loop(0, chunks, project, 0)
+
+    for i in range(1, rows):
+        dest = lax.rem(row + i, rows)
+        x_copy(dest, row).wait_send()
+        y_copy(dest, row).wait_send()
+    for i in range(1, cols):
+        other = lax.rem(col + i, cols)
+        w_copy(other, col).wait_send()
+        f_copy(other, core).wait_send()
+    for j in range(chunks):
+        out_copy(j).wait()
+
+
+def fused(rows, cols, mix_input, gate_logits, w_proj):
+    bf16, f32 = jnp.bfloat16, jnp.float32
+    tokens, gates = mix_input[0], gate_logits[0]
+    tok, features = tokens.shape
+    width_out = gates.shape[1]
+    length = tok * rows
+    width = features // rows
+    table, mixing = channel_table(rows)
+    coarse, fine = base_tables(length)
+    dma = pltpu.SemaphoreType.DMA
+    return pl.pallas_call(
+        functools.partial(fused_kernel, rows, cols, 1.0 / math.sqrt(length * GROUP)),
+        out_shape=jax.ShapeDtypeStruct((tok, width_out), bf16),
+        in_specs=[pl.BlockSpec(memory_space=pl.ANY)] * 7,
+        out_specs=pl.BlockSpec(memory_space=pl.ANY),
+        scratch_shapes=[
+            pltpu.VMEM(tokens.shape, bf16),
+            pltpu.VMEM(gates.shape, bf16),
+            pltpu.VMEM(w_proj.shape, bf16),
+            pltpu.VMEM(table.shape, bf16),
+            pltpu.VMEM(mixing.shape, bf16),
+            pltpu.VMEM(coarse.shape, f32),
+            pltpu.VMEM(fine.shape, f32),
+            pltpu.VMEM((rows, tok, width), bf16),
+            pltpu.VMEM((length, width), bf16),
+            pltpu.VMEM((length // 2, 2 * length), bf16),
+            pltpu.VMEM((2 * length, 2 * width), bf16),
+            pltpu.VMEM((rows, tok, width), bf16),
+            pltpu.VMEM((tok, features), bf16),
+            pltpu.VMEM((cols, *w_proj.shape), bf16),
+            pltpu.VMEM(gates.shape, f32),
+            pltpu.VMEM(gates.shape, bf16),
+            dma((7,)),
+            dma((width_out // OUT_CHUNK,)),
+            dma((rows,)),
+            dma((rows,)),
+            dma((rows,)),
+            dma((rows,)),
+            dma((cols,)),
+            dma((cols,)),
+            dma((cols,)),
+            dma((cols,)),
+        ],
+        compiler_params=pltpu.CompilerParams(
+            collective_id=0, has_side_effects=True, vmem_limit_bytes=48 * 1024 * 1024
+        ),
+    )(
+        tokens,
+        gates,
+        w_proj,
+        jnp.asarray(table, bf16),
+        jnp.asarray(mixing, bf16),
+        jnp.asarray(coarse),
+        jnp.asarray(fine),
+    )[None]
+
+
+def fits(rows, cols, mix_input, gate_logits, w_proj):
+    features = mix_input.shape[2]
+    return (
+        cols == GROUPS
+        and rows == 2 * GROUPS
+        and features == GROUPS * GROUP
+        and w_proj.shape[0] == features
+        and mix_input.shape[0] == cols
+        and mix_input.shape[1] // rows % 128 == 0
+        and mix_input.shape[1] <= 2048
+        and gate_logits.shape[2] % OUT_CHUNK == 0
+    )
+
+
 def solution(mesh):
+    rows, cols = mesh.shape["row"], mesh.shape["col"]
     in_specs = (P("col", "row", None), P("col", "row", None), P("col", None))
     out_specs = P("col", "row", None)
-    return jax.shard_map(
-        on_device, mesh=mesh, in_specs=in_specs, out_specs=out_specs, check_vma=False
-    )
+
+    def run(mix_input, gate_logits, w_proj):
+        body = on_device
+        if fits(rows, cols, mix_input, gate_logits, w_proj):
+            body = functools.partial(fused, rows, cols)
+        return jax.shard_map(
+            body, mesh=mesh, in_specs=in_specs, out_specs=out_specs, check_vma=False
+        )(mix_input, gate_logits, w_proj)
+
+    return run

time: 91.9 us -> 46.1 us (0.50); the launches traced: 90.6 us -> 45.8 us
  Pallas kernels: 0 us -> 37.4 us
  waiting for transfers between devices: 26.3 us -> 0 us
  blocking collectives: 17.9 us -> 0 us
  matrix products: 14.9 us -> 0 us
  between operations: 13.6 us -> 0.02 us
  starting transfers between devices: 6.37 us -> 0 us
  other arithmetic: 2.85 us -> 0 us
    pallas_call x0 -> x1, Pallas kernels: none -> 37.4 us  [fused(): pl.pallas_call(functools.partial(fused_kernel, rows, cols, 1.0 / math.sqr...]
    all_to_all x1 -> x0, waiting for transfers between devices: 25.5 us -> none  [on_device(): lax.all_to_all(packed, 'row', split_axis=1, concat_axis=0, tiled=True)]
    all_to_all x1 -> x0, blocking collectives: 17.9 us -> none  [on_device(): lax.all_to_all(paired, 'row', split_axis=1, concat_axis=0, tiled=True)]
    dot_general x8 -> x0, matrix products: 14.9 us -> none  [the longest x1 4.64 us: on_device(): lax.dot_general(spectrum, lax.all_gather(w_proj, 'col', axis=0, tiled=Tru...]
    unnamed x6 -> x15, local copies, waits for them, and re-layouts: 0.09 us -> 8.35 us
    all_to_all x1 -> x0, starting transfers between devices: 6.37 us -> none  [on_device(): lax.all_to_all(packed, 'row', split_axis=1, concat_axis=0, tiled=True)]
    another operation x2 -> x0, local copies, waits for them, and re-layouts: 2.05 us -> none  [the longest x1 1.51 us: on_device(): pair_re = part_re.reshape(columns // 2, 2, length)]
    add x1 -> x0, local copies, waits for them, and re-layouts: 1.69 us -> none  [position_transform(): second_re = first_re * cos_twist + first_im * sin_twist]
  transfers between devices with their start and end apart: 2 -> 0, of which waited for: 1 -> 0; matrix products, arithmetic and copies ran while one was open for 24% -> 0% of each run, Pallas kernels for 0% -> 0%
where the time goes in v1:
time: 46.1 us; the launch traced here: 45.8 us
  Pallas kernels  37.4 us (81%)
  local copies, waits for them, and re-layouts  8.35 us (18%)
    pallas_call x1, Pallas kernels, fused(): pl.pallas_call(functools.partial(fused_kernel, rows, cols, 1.0 / math.sqr...  37.4 us
    unnamed x15, local copies, waits for them, and re-layouts  8.35 us

profile of v1, /device:TPU:1, one launch (start us, length us, event | category | flops | bytes accessed | tf_op | source)
XLA Modules:
  0.0 45.8 jit_solution(12756793972825775494)
XLA Ops:
  0.0 0.0 copy-start
  0.0 1.2 %copy-done = bf16[1,256,2048]{2,1,0:T(8,128)(2,1)S(1)} copy-done((bf16[1,256,2048]{2,1,0:T(8,128)(2,1)S(1)}, bf16[1,256,2048]{2,1,0:T(8,128)(2,1)}, u32[]{:S(2)}) %copy-start) | copy-done | bytes 1048600
  1.2 0.0 copy-start.1
  1.2 1.2 %copy-done.1 = bf16[256,2048]{1,0:T(8,128)(2,1)S(1)} copy-done((bf16[256,2048]{1,0:T(8,128)(2,1)S(1)}, bf16[256,2048]{1,0:T(8,128)(2,1)}, u32[]{:S(2)}) %copy-start.1) | copy-done | bytes 1048600
  2.5 0.0 copy-start.2
  2.5 1.0 %copy-done.2 = bf16[1,256,1024]{2,1,0:T(8,128)(2,1)S(1)} copy-done((bf16[1,256,1024]{2,1,0:T(8,128)(2,1)S(1)}, bf16[1,256,1024]{2,1,0:T(8,128)(2,1)}, u32[]{:S(2)}) %copy-start.2) | copy-done | bytes 524312
  3.5 0.0 copy-start.3
  3.5 1.0 %copy-done.3 = f32[2,32,2048]{2,1,0:T(8,128)S(1)} copy-done((f32[2,32,2048]{2,1,0:T(8,128)S(1)}, f32[2,32,2048]{2,1,0:T(8,128)}, u32[]{:S(2)}) %copy-start.3) | copy-done | bytes 524312
  4.5 0.0 copy-start.4
  4.5 1.0 %copy-done.4 = f32[2,32,2048]{2,1,0:T(8,128)S(1)} copy-done((f32[2,32,2048]{2,1,0:T(8,128)S(1)}, f32[2,32,2048]{2,1,0:T(8,128)}, u32[]{:S(2)}) %copy-start.4) | copy-done | bytes 524312
  5.6 0.0 copy-start.5
  5.6 0.9 %copy-done.5 = bf16[256,256]{1,0:T(8,128)(2,1)S(1)} copy-done((bf16[256,256]{1,0:T(8,128)(2,1)S(1)}, bf16[256,256]{1,0:T(8,128)(2,1)}, u32[]{:S(2)}) %copy-start.5) | copy-done | bytes 131096
  6.5 0.0 copy-start.6
  6.5 0.9 %copy-done.6 = bf16[256,256]{1,0:T(8,128)(2,1)S(1)} copy-done((bf16[256,256]{1,0:T(8,128)(2,1)S(1)}, bf16[256,256]{1,0:T(8,128)(2,1)}, u32[]{:S(2)}) %copy-start.6) | copy-done | bytes 131096
  7.4 37.4 %shard_map.73 = bf16[256,2048]{1,0:T(8,128)(2,1)S(1)} custom-call(bf16[256,1024]{1,0:T(8,128)(2,1)S(1)} %bitcast.5, bf16[256,2048]{1,0:T(8,128)(2,1)S(1)} %bitcast.4, bf16[256,2048]{1,0:T(8,128)(2,1)S(1)} %copy-done.1, bf16[256,256]{1,0:T(8,128)(2,1)S(1)} %copy-done.6, bf16[256,256]{1,0:T(8,128)(2,1)S(1)} %copy-done.5, f32[2,32,2048]{2,1,0:T(8,128)S(1)} %copy-done.4, ...), custom_call_target="tpu_custom_call" | custom-call | tf_op jit(solution)/shard_map/pallas_call | solution.py:403
  44.8 1.0 %copy.9 = bf16[1,256,2048]{2,1,0:T(8,128)(2,1)} copy(bf16[1,256,2048]{2,1,0:T(8,128)(2,1)S(1)} %bitcast.3) | data formatting | bytes 2097152
Async XLA Ops:
  0.0 1.2 %copy-start = (bf16[1,256,2048]{2,1,0:T(8,128)(2,1)S(1)}, bf16[1,256,2048]{2,1,0:T(8,128)(2,1)}, u32[]{:S(2)}) copy-start(bf16[1,256,2048]{2,1,0:T(8,128)(2,1)} %param.8) | copy-start | bytes 3145732
  1.2 1.2 %copy-start.1 = (bf16[256,2048]{1,0:T(8,128)(2,1)S(1)}, bf16[256,2048]{1,0:T(8,128)(2,1)}, u32[]{:S(2)}) copy-start(bf16[256,2048]{1,0:T(8,128)(2,1)} %w_hbm.1) | copy-start | bytes 3145732
  2.5 1.0 %copy-start.2 = (bf16[1,256,1024]{2,1,0:T(8,128)(2,1)S(1)}, bf16[1,256,1024]{2,1,0:T(8,128)(2,1)}, u32[]{:S(2)}) copy-start(bf16[1,256,1024]{2,1,0:T(8,128)(2,1)} %param.7) | copy-start | bytes 1572868
  3.5 1.0 %copy-start.3 = (f32[2,32,2048]{2,1,0:T(8,128)S(1)}, f32[2,32,2048]{2,1,0:T(8,128)}, u32[]{:S(2)}) copy-start(f32[2,32,2048]{2,1,0:T(8,128)} %constant.11.clone.fine_hbm) | copy-start | bytes 1572868
  4.5 1.0 %copy-start.4 = (f32[2,32,2048]{2,1,0:T(8,128)S(1)}, f32[2,32,2048]{2,1,0:T(8,128)}, u32[]{:S(2)}) copy-start(f32[2,32,2048]{2,1,0:T(8,128)} %constant.10.clone.coarse_hbm) | copy-start | bytes 1572868
  5.6 0.9 %copy-start.5 = (bf16[256,256]{1,0:T(8,128)(2,1)S(1)}, bf16[256,256]{1,0:T(8,128)(2,1)}, u32[]{:S(2)}) copy-start(bf16[256,256]{1,0:T(8,128)(2,1)} %constant.9.clone.mix_hbm) | copy-start | bytes 393220
  6.5 0.9 %copy-start.6 = (bf16[256,256]{1,0:T(8,128)(2,1)S(1)}, bf16[256,256]{1,0:T(8,128)(2,1)}, u32[]{:S(2)}) copy-start(bf16[256,256]{1,0:T(8,128)(2,1)} %constant.8.clone.chan_hbm) | copy-start | bytes 393220

commit v2 on v1

--- a/solution.py
+++ b/solution.py
@@ -96,21 +96,24 @@
     return (gate_open * projected).astype(jnp.bfloat16)[None]
 
 
-def channel_table(rows):
-    half = GROUP // 2
-    quarter = half // 2
-    table = np.zeros((GROUP, GROUP))
+def channel_table():
+    half, part = GROUP // 2, GROUP // 8
+    table = np.zeros((2, GROUP, GROUP))
     mixing = np.zeros((GROUP, GROUP))
     channel = np.arange(GROUP)
-    for core in range(2):
-        for i in range(quarter):
-            m = quarter * core + i
-            low, high = half * core + i, half * core + quarter + i
-            angle = 2.0 * np.pi * (channel * m % GROUP) / GROUP
-            table[:, low] = np.cos(angle)
-            table[:, high] = np.sin(angle) if m else np.cos(np.pi * channel)
-            mixing[low, m] = 1.0
-            mixing[high, GROUP - m if m else half] = 1.0
+    for stage in range(2):
+        for core in range(2):
+            for i in range(part):
+                m = 2 * part * core + part * stage + i
+                angle = 2.0 * np.pi * (channel * m % GROUP) / GROUP
+                pair = (np.cos(angle), np.sin(angle) if m else np.cos(np.pi * channel))
+                for which in range(2):
+                    at = half * stage + part * which + i
+                    table[0, :, at + 2 * part * core] = pair[which]
+                    table[1, :, at + 2 * part * (1 - core)] = pair[which]
+                low = half * stage + 2 * part * core + i
+                mixing[low, m] = 1.0
+                mixing[low + part, GROUP - m if m else half] = 1.0
     return table, mixing
 
 
@@ -151,9 +154,11 @@
     tab,
     rhs,
     send_y,
+    recv_y,
     spec,
     wall,
     sig,
+    acc,
     outv,
     load_sem,
     out_sem,
@@ -170,10 +175,11 @@
     row, col = lax.axis_index("row"), lax.axis_index("col")
     chip, core = row // 2, row % 2
     tok = xv.shape[0]
-    width = recv_x.shape[1]
-    length = recv_x.shape[0]
+    half_tok = tok // 2
+    lanes = recv_x.shape[3]
+    length = tok * rows
     half_len = length // 2
-    half_rows = GROUP // 2
+    upper = row // (rows // 2)
 
     loads = [
         pltpu.make_async_copy(src, dst, load_sem.at[i])
@@ -202,35 +208,40 @@
             barrier, inc=1, device_id=(row, lax.rem(col + i, cols)), device_id_type=MESH
         )
 
-    def x_copy(dest, source):
+    def x_copy(h, dest, source):
         return pltpu.make_async_remote_copy(
-            src_ref=send_x.at[dest],
-            dst_ref=recv_x.at[pl.ds(pl.multiple_of(source * tok, tok), tok), :],
-            send_sem=sx.at[dest],
-            recv_sem=rx.at[source],
+            src_ref=send_x.at[h, dest],
+            dst_ref=recv_x.at[h, source],
+            send_sem=sx.at[h, dest],
+            recv_sem=rx.at[h, source],
             device_id=(dest, col),
             device_id_type=MESH,
         )
 
-    def y_copy(dest, source):
+    def y_copy(h, dest, source):
         return pltpu.make_async_remote_copy(
-            src_ref=send_y.at[dest],
-            dst_ref=spec.at[:, pl.ds(pl.multiple_of(source * width, width), width)],
-            send_sem=sy.at[dest],
-            recv_sem=ry.at[source],
+            src_ref=send_y.at[h, dest],
+            dst_ref=recv_y.at[h, source],
+            send_sem=sy.at[h, dest],
+            recv_sem=ry.at[h, source],
             device_id=(dest, col),
             device_id_type=MESH,
         )
 
     def w_part(owner, part):
-        return wall.at[owner, pl.ds(pl.multiple_of(part * half_rows, half_rows), half_rows), :]
-
-    def w_copy(dest, owner):
+        return wall.at[part, pl.ds(pl.multiple_of(owner * lanes, lanes), lanes), :]
+
+    def w_piece(owner, piece):
+        size = lanes // 2
+        start = pl.multiple_of(owner * lanes + piece * size, size)
+        return wall.at[core, pl.ds(start, size), :]
+
+    def w_copy(dest, owner, slot, piece):
         return pltpu.make_async_remote_copy(
-            src_ref=w_part(owner, core),
-            dst_ref=w_part(owner, core),
-            send_sem=sw.at[dest],
-            recv_sem=rw.at[owner],
+            src_ref=w_piece(owner, piece),
+            dst_ref=w_piece(owner, piece),
+            send_sem=sw.at[slot, piece],
+            recv_sem=rw.at[owner, piece],
             device_id=(row, dest),
             device_id_type=MESH,
         )
@@ -245,35 +256,48 @@
             device_id_type=MESH,
         )
 
+    col_x = col + 1 - 2 * (col % 2)
+    col_y = lax.rem(col + 2, cols)
+    col_far = lax.rem(col_x + 2, cols)
+    relay_from = jnp.where(core == 0, col_x, col_y)
+    relay_to = jnp.where(core == 0, col_y, col_x)
+    low_lanes = lax.broadcasted_iota(jnp.int32, (half_tok, lanes), 1) < lanes // 2
+
+    def channel_stage(h, carry):
+        to = pl.ds(pl.multiple_of(h * lanes, lanes), lanes)
+        for g in range(GROUPS):
+            at = slice(g * GROUP, (g + 1) * GROUP)
+            top = jnp.dot(xv[:half_tok, at], chan[0, :, to], preferred_element_type=f32)
+            low = jnp.dot(xv[half_tok:, at], chan[1, :, to], preferred_element_type=f32)
+            for part in range(2):
+                pick = low_lanes if part == 0 else jnp.logical_not(low_lanes)
+                send_x[h, 2 * g + part] = jnp.where(pick, top, low).astype(bf16)
+        recv_x[h, row] = send_x[h, row]
+        return carry
+
+    def send_stage(h):
+        for i in range(rows):
+            dest = lax.rem(2 * chip + rows // 2 + i, rows)
+
+            @pl.when(dest != row)
+            def _():
+                x_copy(h, dest, row).start()
+
     loads[0].wait()
     loads[1].wait()
-    pl.semaphore_wait(barrier, rows - 1 + cols - 1)
-
-    for i in range(GROUPS):
-        g = lax.rem(chip + GROUPS // 2 + i, GROUPS)
-        packed = jnp.dot(
-            xv[:, pl.ds(pl.multiple_of(g * GROUP, GROUP), GROUP)],
-            chan[...],
-            preferred_element_type=f32,
-        ).astype(bf16)
-        for part in range(2):
-            dest = 2 * g + part
-            block = packed[:, part * width : (part + 1) * width]
-
-            @pl.when(dest != row)
-            def _():
-                send_x[dest] = block
-                x_copy(dest, row).start()
-
-            @pl.when(dest == row)
-            def _():
-                recv_x[pl.ds(pl.multiple_of(row * tok, tok), tok), :] = block
-
+    channel_stage(0, 0)
     loads[2].wait()
     loads[3].wait()
-    wall[col] = jnp.dot(mix[...], wv[...], preferred_element_type=f32).astype(bf16)
-    for i in range(1, cols):
-        w_copy(lax.rem(col + i, cols), col).start()
+    mixed_w = jnp.dot(mix[...], wv[...], preferred_element_type=f32).astype(bf16)
+    for h in range(2):
+        w_part(col, h)[...] = mixed_w[h * lanes : (h + 1) * lanes]
+    pl.semaphore_wait(barrier, rows - 1 + cols - 1)
+    send_stage(0)
+    for piece in range(2):
+        w_copy(col_x, col, 0, piece).start()
+        w_copy(col_y, col, 1, piece).start()
+    channel_stage(1, 0)
+    send_stage(1)
 
     loads[4].wait()
     loads[5].wait()
@@ -291,6 +315,93 @@
 
     lax.fori_loop(0, half_len // TAB_STEP, make_rows, 0)
 
+    quarter = lanes // 4
+    left = lax.broadcasted_iota(jnp.int32, (lanes, lanes), 0)
+    right = lax.broadcasted_iota(jnp.int32, (lanes, lanes), 1)
+    slot = right % (2 * quarter)
+    odd = lax.broadcasted_iota(jnp.int32, (half_tok, lanes), 0) % 2 == 1
+    flip = jnp.where(jnp.logical_and(odd, jnp.logical_not(low_lanes)), -1.0, 1.0)
+
+    def position_stage(h):
+        first = jnp.logical_and(core == 0, slot % quarter == 0)
+        if h > 0:
+            first = jnp.logical_and(first, slot < 0)
+        cos_from = jnp.where(first, slot, slot % quarter)
+        sin_from = slot % quarter + quarter
+        sign = jnp.where(first, 0.0, jnp.where(slot < quarter, -1.0, 1.0))
+        picks = []
+        for part in range(2):
+            offset = 2 * quarter * jnp.where(core == part, 0, 1)
+            picks.append(
+                (
+                    jnp.where(left == cos_from + offset, 1.0, 0.0).astype(bf16),
+                    jnp.where(left == sin_from + offset, sign, 0.0).astype(bf16),
+                )
+            )
+
+        for i in range(rows):
+            source = lax.rem(row + i, rows)
+
+            @pl.when(source != row)
+            def _():
+                x_copy(h, source, source).wait_recv()
+
+            block = recv_x[h, source]
+            for part in range(2):
+                for which in range(2):
+                    picked = jnp.dot(block, picks[part][which], preferred_element_type=f32)
+                    start = which * length + source * tok + part * half_tok
+                    to = pl.ds(pl.multiple_of(start, half_tok), half_tok)
+                    rhs[h, to, :] = (picked * flip).astype(bf16)
+
+        def position_block(e, carry):
+            at = pl.ds(pl.multiple_of(e * tok, tok), tok)
+            block = jnp.dot(tab[at, :], rhs[h], preferred_element_type=f32) * norm_factor
+            top = block[:half_tok]
+            low = pltpu.roll(block[half_tok:], lanes // 2, 1)
+            for part in range(2):
+                dest = e + part * (rows // 2)
+                pick = low_lanes if part == 0 else jnp.logical_not(low_lanes)
+                piece = jnp.where(pick, top, low).astype(bf16)
+
+                @pl.when(dest != row)
+                def _():
+                    send_y[h, dest] = piece
+                    y_copy(h, dest, row).start()
+
+                @pl.when(dest == row)
+                def _():
+                    recv_y[h, row] = piece
+
+            return carry
+
+        lax.fori_loop(0, rows // 2, position_block, 0)
+
+    def collect(h):
+        for i in range(1, rows):
+            source = lax.rem(row + i, rows)
+            y_copy(h, source, source).wait_recv()
+        for g in range(GROUPS):
+            one = recv_y[h, 2 * g].astype(f32)
+            two = recv_y[h, 2 * g + 1].astype(f32)
+            kept = jnp.where(low_lanes, one, pltpu.roll(two, lanes // 2, 1)).astype(bf16)
+            moved = jnp.where(low_lanes, pltpu.roll(one, lanes // 2, 1), two).astype(bf16)
+            to = slice(g * lanes, (g + 1) * lanes)
+            spec[h, pl.ds(pl.multiple_of(upper * half_tok, half_tok), half_tok), to] = kept
+            spec[h, pl.ds(pl.multiple_of((1 - upper) * half_tok, half_tok), half_tok), to] = moved
+
+    w_copy(relay_from, relay_from, 0, 0).wait_recv()
+    w_copy(relay_to, relay_from, 2, 0).start()
+    position_stage(0)
+    w_copy(relay_from, relay_from, 0, 1).wait_recv()
+    w_copy(relay_to, relay_from, 2, 1).start()
+    for piece in range(2):
+        w_copy(relay_to, relay_to, 1, piece).wait_recv()
+    f_copy(col_x, core).start()
+    f_copy(col_y, core).start()
+
+    position_stage(1)
+
     loads[6].wait()
 
     def open_gate(i, carry):
@@ -300,78 +411,35 @@
 
     lax.fori_loop(0, tok // 16, open_gate, 0)
 
-    quarter = width // 2
-    left = lax.broadcasted_iota(jnp.int32, (width, width), 0)
-    right = lax.broadcasted_iota(jnp.int32, (width, width), 1)
-    first = jnp.logical_and(core == 0, right % quarter == 0)
-    cos_from = jnp.where(first, right, right % quarter)
-    cos_pick = jnp.where(left == cos_from, 1.0, 0.0).astype(bf16)
-    sign = jnp.where(first, 0.0, jnp.where(right < quarter, -1.0, 1.0))
-    sin_pick = jnp.where(left == right % quarter + quarter, sign, 0.0).astype(bf16)
-    odd = lax.broadcasted_iota(jnp.int32, (tok, width), 0) % 2
-    flip = jnp.where(odd == 1, -1.0, 1.0)
-
-    for i in range(rows):
-        source = lax.rem(row + i, rows)
-
-        @pl.when(source != row)
-        def _():
-            x_copy(source, source).wait_recv()
-
-        at = pl.ds(pl.multiple_of(source * tok, tok), tok)
-        block = recv_x[at, :]
-        for base, pick in ((0, cos_pick), (length, sin_pick)):
-            picked = jnp.dot(block, pick, preferred_element_type=f32)
-            to = pl.ds(pl.multiple_of(base + source * tok, tok), tok)
-            rhs[to, :width] = picked.astype(bf16)
-            rhs[to, width:] = (picked * flip).astype(bf16)
-
-    def position_block(e, carry):
-        at = pl.ds(pl.multiple_of(e * tok, tok), tok)
-        block = jnp.dot(tab[at, :], rhs[...], preferred_element_type=f32) * norm_factor
-        block = block.astype(bf16)
-        for part in range(2):
-            dest = e + part * (rows // 2)
-            piece = block[:, part * width : (part + 1) * width]
-
-            @pl.when(dest != row)
-            def _():
-                send_y[dest] = piece
-                y_copy(dest, row).start()
-
-            @pl.when(dest == row)
-            def _():
-                spec[:, pl.ds(pl.multiple_of(row * width, width), width)] = piece
-
+    for piece in range(2):
+        w_copy(col_far, col_far, 2, piece).wait_recv()
+    f_copy(col_far, core).start()
+
+    chunks = outv.shape[1] // OUT_CHUNK
+
+    def chunk_at(j):
+        return pl.ds(pl.multiple_of(j * OUT_CHUNK, OUT_CHUNK), OUT_CHUNK)
+
+    def out_copy(j):
+        return pltpu.make_async_copy(
+            outv.at[:, chunk_at(j)], out_hbm.at[:, chunk_at(j)], out_sem.at[j]
+        )
+
+    collect(0)
+    for owner in (col_x, col_y, col_far):
+        f_copy(owner, 1 - core).wait_recv()
+
+    def project_first(j, carry):
+        at = chunk_at(j)
+        acc[:, at] = jnp.dot(spec[0], wall[0, :, at], preferred_element_type=f32)
         return carry
 
-    lax.fori_loop(0, rows // 2, position_block, 0)
-
-    for i in range(1, cols):
-        owner = lax.rem(col + i, cols)
-        w_copy(owner, owner).wait_recv()
-        f_copy(owner, core).start()
-
-    for i in range(1, rows):
-        source = lax.rem(row + i, rows)
-        y_copy(source, source).wait_recv()
-    for i in range(1, cols):
-        owner = lax.rem(col + i, cols)
-        f_copy(owner, 1 - core).wait_recv()
-
-    chunks = outv.shape[1] // OUT_CHUNK
-
-    def out_copy(j):
-        at = pl.ds(pl.multiple_of(j * OUT_CHUNK, OUT_CHUNK), OUT_CHUNK)
-        return pltpu.make_async_copy(outv.at[:, at], out_hbm.at[:, at], out_sem.at[j])
+    lax.fori_loop(0, chunks, project_first, 0)
+    collect(1)
 
     def project(j, carry):
-        at = pl.ds(pl.multiple_of(j * OUT_CHUNK, OUT_CHUNK), OUT_CHUNK)
-        total = jnp.zeros((tok, OUT_CHUNK), f32)
-        for g in range(GROUPS):
-            total += jnp.dot(
-                spec[:, g * GROUP : (g + 1) * GROUP], wall[g, :, at], preferred_element_type=f32
-            )
+        at = chunk_at(j)
+        total = acc[:, at] + jnp.dot(spec[1], wall[1, :, at], preferred_element_type=f32)
         outv[:, at] = (sig[:, at] * total).astype(bf16)
         out_copy(j).start()
         return carry
@@ -380,12 +448,15 @@
 
     for i in range(1, rows):
         dest = lax.rem(row + i, rows)
-        x_copy(dest, row).wait_send()
-        y_copy(dest, row).wait_send()
-    for i in range(1, cols):
-        other = lax.rem(col + i, cols)
-        w_copy(other, col).wait_send()
-        f_copy(other, core).wait_send()
+        for h in range(2):
+            x_copy(h, dest, row).wait_send()
+            y_copy(h, dest, row).wait_send()
+    for piece in range(2):
+        w_copy(col_x, col, 0, piece).wait_send()
+        w_copy(col_y, col, 1, piece).wait_send()
+        w_copy(relay_to, relay_from, 2, piece).wait_send()
+    for owner in (col_x, col_y, col_far):
+        f_copy(owner, core).wait_send()
     for j in range(chunks):
         out_copy(j).wait()
 
@@ -397,7 +468,7 @@
     width_out = gates.shape[1]
     length = tok * rows
     width = features // rows
-    table, mixing = channel_table(rows)
+    table, mixing = channel_table()
     coarse, fine = base_tables(length)
     dma = pltpu.SemaphoreType.DMA
     return pl.pallas_call(
@@ -413,28 +484,30 @@
             pltpu.VMEM(mixing.shape, bf16),
             pltpu.VMEM(coarse.shape, f32),
             pltpu.VMEM(fine.shape, f32),
-            pltpu.VMEM((rows, tok, width), bf16),
-            pltpu.VMEM((length, width), bf16),
+            pltpu.VMEM((2, rows, tok // 2, width), bf16),
+            pltpu.VMEM((2, rows, tok // 2, width), bf16),
             pltpu.VMEM((length // 2, 2 * length), bf16),
-            pltpu.VMEM((2 * length, 2 * width), bf16),
-            pltpu.VMEM((rows, tok, width), bf16),
-            pltpu.VMEM((tok, features), bf16),
-            pltpu.VMEM((cols, *w_proj.shape), bf16),
+            pltpu.VMEM((2, 2 * length, width), bf16),
+            pltpu.VMEM((2, rows, tok // 2, width), bf16),
+            pltpu.VMEM((2, rows, tok // 2, width), bf16),
+            pltpu.VMEM((2, tok, features // 2), bf16),
+            pltpu.VMEM((2, features // 2, width_out), bf16),
+            pltpu.VMEM(gates.shape, f32),
             pltpu.VMEM(gates.shape, f32),
             pltpu.VMEM(gates.shape, bf16),
             dma((7,)),
             dma((width_out // OUT_CHUNK,)),
-            dma((rows,)),
-            dma((rows,)),
-            dma((rows,)),
-            dma((rows,)),
-            dma((cols,)),
-            dma((cols,)),
+            dma((2, rows)),
+            dma((2, rows)),
+            dma((2, rows)),
+            dma((2, rows)),
+            dma((3, 2)),
+            dma((cols, 2)),
             dma((cols,)),
             dma((cols,)),
         ],
         compiler_params=pltpu.CompilerParams(
-            collective_id=0, has_side_effects=True, vmem_limit_bytes=48 * 1024 * 1024
+            collective_id=0, has_side_effects=True, vmem_limit_bytes=67043328
         ),
     )(
         tokens,
@@ -454,8 +527,9 @@
         and rows == 2 * GROUPS
         and features == GROUPS * GROUP
         and w_proj.shape[0] == features
+        and features // rows == 128
         and mix_input.shape[0] == cols
-        and mix_input.shape[1] // rows % 128 == 0
+        and mix_input.shape[1] // rows % 256 == 0
         and mix_input.shape[1] <= 2048
         and gate_logits.shape[2] % OUT_CHUNK == 0
     )

time: 46.1 us -> 33.3 us (0.72)
  Pallas kernels: 37.4 us -> 30.8 us
  local copies, waits for them, and re-layouts: 8.35 us -> 2.3 us
    pallas_call x1, Pallas kernels: 37.4 us -> 30.8 us  [fused(): pl.pallas_call(functools.partial(fused_kernel, rows, cols, 1.0 / math.sqr...]
    unnamed x15 -> x1, local copies, waits for them, and re-layouts: 8.35 us -> 2.3 us
where the time goes in v2:
time: 33.3 us; the launch traced here: 33.1 us
  Pallas kernels  30.8 us (92%)
  local copies, waits for them, and re-layouts  2.3 us (7%)
    pallas_call x1, Pallas kernels, fused(): pl.pallas_call(functools.partial(fused_kernel, rows, cols, 1.0 / math.sqr...  30.8 us
    unnamed x1, local copies, waits for them, and re-layouts  2.3 us

profile of v2, /device:TPU:1, one launch (start us, length us, event | category | flops | bytes accessed | tf_op | source)
XLA Modules:
  0.0 33.1 jit_solution(5590043959633758861)
XLA Ops:
  0.0 30.8 %shard_map.73 = bf16[256,2048]{1,0:T(8,128)(2,1)} custom-call(bf16[256,1024]{1,0:T(8,128)(2,1)} %bitcast.5, bf16[256,2048]{1,0:T(8,128)(2,1)} %bitcast.4, bf16[256,2048]{1,0:T(8,128)(2,1)} %w_hbm.1, bf16[2,256,256]{2,1,0:T(8,128)(2,1)} %constant.8.clone.chan_hbm, bf16[256,256]{1,0:T(8,128)(2,1)} %constant.9.clone.mix_hbm, ...), custom_call_target="tpu_custom_call" | custom-call | tf_op jit(solution)/shard_map/pallas_call | solution.py:474
  30.8 2.3 %copy.9 = bf16[1,256,2048]{2,1,0:T(8,128)(2,1)} copy(bf16[1,256,2048]{2,1,0:T(8,128)(2,1)} %bitcast.3) | data formatting | bytes 2097152
